TPU v7x, 256 devices: a whole 4x4x8 slice. The times are simulated.
256 devices in a mesh: rep: 2 (over z_hi), fs: 16 (over z_lo, x), tp: 8 (over y, core).
Axes of the slice: x: 4, y: 4, z: 8 (z_hi: 2, z_lo: 4; z = z_hi * 4 + z_lo), core: 2. Of those that a mesh axis runs over, the one named last changes fastest.
Arguments:
- tokens: bfloat16 [32768, 2048], P(('rep', 'fs'), 'tp'), may hold values from -6 to 6
- mix_in_gain: bfloat16 [2048], replicated, may hold values from 0.099609375 to 1.8984375
- bgate_weight: bfloat16 [2048, 2048], P('fs', 'tp'), may hold values from -0.125 to 0.125
- cgate_weight: bfloat16 [2048, 2048], P('fs', 'tp'), may hold values from -0.125 to 0.125
- value_weight: bfloat16 [2048, 2048], P('fs', 'tp'), may hold values from -0.125 to 0.125
- conv_taps: bfloat16 [3, 2048], replicated, may hold values from -3 to 3
- out_weight: bfloat16 [2048, 2048], P('tp', 'fs'), may hold values from -0.41984465 to 0.41984465
- mix_out_gain: bfloat16 [2048], replicated, may hold values from 0.099609375 to 1.8984375
- ffn_in_gain: bfloat16 [2048], replicated, may hold values from 0.099609375 to 1.8984375
- up_weight: bfloat16 [2048, 8192], P('fs', 'tp'), may hold values from -0.125 to 0.125
- down_weight: bfloat16 [8192, 2048], P('tp', 'fs'), may hold values from -0.20992233 to 0.20992233
- ffn_out_gain: bfloat16 [2048], replicated, may hold values from 0.099609375 to 1.8984375
Outputs:
- result: bfloat16 [32768, 2048], P(('rep', 'fs'), 'tp')
All inputs are finite; a program needn't handle non-finite values.
Results may differ from a plain program's by a relative error of at most 0.02.
Values may be sent and summed in bfloat16 or wider, within the bound.
A program may use at most 128 MiB of HBM per device.

v0:
```python
import jax
import jax.numpy as jnp
from jax import lax
from jax.sharding import Mesh
from jax.sharding import PartitionSpec as P

LEN = 256
FS = ("fs_0", "fs_1")
REP_FS = ("rep", "fs_0", "fs_1")
epsilon = 1e-06


def in_order(pieces, dim):
    pieces = jnp.moveaxis(pieces, 0, dim)
    shape = pieces.shape
    return pieces.reshape(*shape[:dim], shape[dim] * shape[dim + 1], *shape[dim + 2 :])


def from_everyone(x, axis):
    length = lax.axis_size(axis)
    return lax.all_to_all(jnp.broadcast_to(x[None], (length, *x.shape)), axis, 0, 0, tiled=True)


def gathered_copies(x, axis, dim):
    return in_order(from_everyone(x, axis), dim)


def in_blocks(x, dim, length):
    before, after = (x.shape[:dim], x.shape[dim + 1 :])
    return jnp.moveaxis(x.reshape(*before, length, -1, *after), dim, 0)


def sent_and_summed(x, axis, dim):
    pieces = in_blocks(x, dim, lax.axis_size(axis))
    arrived = lax.all_to_all(pieces, axis, split_axis=0, concat_axis=0, tiled=True)
    return arrived.astype(jnp.float32).sum(axis=0)


def of_everyone(x, axis):
    everything = from_everyone(x, axis)
    return jnp.sum(everything, axis=0)


def all_blocks(x, axes, order):
    pieces = x
    for k in order:
        pieces = lax.all_gather(pieces, axes[k])
    done = order[::-1]
    back = [done.index(k) for k in range(len(axes))]
    pieces = pieces.transpose(*back, *range(len(axes), pieces.ndim))
    return pieces.reshape(-1, *x.shape)


def whole_of(x, axes, order, dim):
    return in_order(all_blocks(x, axes, order), dim)


def normalize(rows, gain):
    rows = rows.astype(jnp.float32)
    factor = lax.rsqrt(jnp.mean(rows * rows, axis=-1, keepdims=True) + epsilon)
    return rows * factor * gain.astype(jnp.float32)


def convolve(inner, taps):
    seqs = inner.reshape(-1, LEN, inner.shape[1])
    padded = jnp.pad(seqs, ((0, 0), (1, 1), (0, 0)))
    weights = taps.astype(jnp.float32)
    out = weights[0] * padded[:, :-2] + weights[1] * padded[:, 1:-1] + weights[2] * padded[:, 2:]
    return out.reshape(inner.shape)


def body(
    tokens,
    mix_in_gain,
    bgate_weight,
    cgate_weight,
    value_weight,
    conv_taps,
    out_weight,
    mix_out_gain,
    ffn_in_gain,
    up_weight,
    down_weight,
    ffn_out_gain,
):
    column = lax.axis_index("tp")
    own_width = tokens.shape[1]
    first = column * own_width
    full_width = mix_in_gain.shape[0]
    whole = lax.all_gather(tokens, "tp", axis=1, tiled=True)
    normed = normalize(whole, mix_in_gain).astype(jnp.bfloat16)

    def add_rows(piece):
        return jnp.dot(normed, piece, preferred_element_type=jnp.float32)

    bgate = add_rows(gathered_copies(bgate_weight, FS, 0))
    cgate = add_rows(gathered_copies(cgate_weight, FS, 0))
    value = add_rows(gathered_copies(value_weight, FS, 0))
    bgate = bgate.astype(jnp.bfloat16)
    cgate = cgate.astype(jnp.bfloat16)
    value = value.astype(jnp.bfloat16)
    channels = bgate.shape[1]
    own_taps = lax.dynamic_slice_in_dim(conv_taps, column * channels, channels, 1)
    inner = cgate.astype(jnp.float32) * value.astype(jnp.float32)
    gated = (bgate.astype(jnp.float32) * convolve(inner, own_taps)).astype(jnp.bfloat16)
    partial_mix = jnp.dot(
        gated, gathered_copies(out_weight, FS, 1), preferred_element_type=jnp.float32
    )
    mixed = sent_and_summed(partial_mix.astype(jnp.bfloat16), "tp", 1)
    power = of_everyone(jnp.sum(mixed * mixed, axis=1), "tp")
    gain_own = lax.dynamic_slice_in_dim(mix_out_gain, first, own_width, 0).astype(jnp.float32)
    scaled = mixed * lax.rsqrt(power[:, None] / full_width + epsilon) * gain_own
    resid_own = (tokens.astype(jnp.float32) + scaled).astype(jnp.bfloat16)
    resid = lax.all_gather(resid_own, "tp", axis=1, tiled=True)
    second = normalize(resid, ffn_in_gain).astype(jnp.bfloat16)
    lifted = jnp.dot(second, whole_of(up_weight, FS, (0, 1), 0), preferred_element_type=jnp.float32)
    active = jnp.square(jnp.maximum(lifted, 0.0)).astype(jnp.bfloat16)
    partial_ffn = jnp.dot(
        active, whole_of(down_weight, FS, (0, 1), 1), preferred_element_type=jnp.float32
    )
    ffn = sent_and_summed(partial_ffn.astype(jnp.bfloat16), "tp", 1)
    ffn_energy = of_everyone(jnp.sum(ffn * ffn, axis=1), "tp")
    out_gain = lax.dynamic_slice_in_dim(ffn_out_gain, first, own_width, 0).astype(jnp.float32)
    closing = ffn * lax.rsqrt(ffn_energy[:, None] / full_width + epsilon) * out_gain
    return (resid_own.astype(jnp.float32) + closing).astype(jnp.bfloat16)


def solution(mesh):
    torus = Mesh(
        mesh.devices.reshape(mesh.shape["rep"], 4, 4, mesh.shape["tp"]),
        ("rep", "fs_0", "fs_1", "tp"),
    )
    return jax.shard_map(
        body,
        mesh=torus,
        in_specs=(
            P(REP_FS, "tp"),
            P(),
            P(FS, "tp"),
            P(FS, "tp"),
            P(FS, "tp"),
            P(),
            P("tp", FS),
            P(),
            P(),
            P(FS, "tp"),
            P("tp", FS),
            P(),
        ),
        out_specs=P(REP_FS, "tp"),
        check_vma=False,
    )
```

profile of v0, /device:TPU:1, one launch (start us, length us, event | category | flops | bytes accessed | tf_op | source)
XLA Modules:
  0.0 391.8 jit_solution(6726258593251835402)
XLA Ops:
  8.8 36.9 %all-gather.19.cloned.1.call-done = bf16[4096,128]{1,0:T(8,128)(2,1)} async-done(((bf16[1024,128]{1,0:T(8,128)(2,1)}), bf16[4096,128]{1,0:T(8,128)(2,1)}) %all-gather.19.cloned.1.call-update) | async-done | bytes 1048592 | tf_op jit(solution)/shard_map/all_gather | solution.py:47
  45.8 0.9 broadcast_in_dim.13
  46.7 40.9 %all_to_all.42 = bf16[16,128,256]{2,1,0:T(8,128)(2,1)S(1)} all-to-all(bf16[16,128,256]{2,1,0:T(8,128)(2,1)S(1)} %broadcast_in_dim.13), channel_id=1, replica_groups=mesh['rep'=2,'fs_0'=4,'fs_1'=4,'tp'=8] {'fs_0','fs_1'}, dimensions={0} | all-to-all | bytes 2097152 | tf_op jit(solution)/shard_map/all_to_all | solution.py:21
  87.6 1.1 broadcast_in_dim.14
  88.7 9.8 %all-to-all-start.2 = ((bf16[16,128,256]{2,1,0:T(8,128)(2,1)}), bf16[16,128,256]{2,1,0:T(8,128)(2,1)S(1)}, u32[]{:S(2)}, u32[]{:S(2)}) async-start(bf16[16,128,256]{2,1,0:T(8,128)(2,1)} %broadcast_in_dim.14), calls=%async_computation.2 | async-start | bytes 2097152 | tf_op jit(solution)/shard_map/all_to_all | solution.py:21
  98.6 21.9 %all-to-all-done.2 = bf16[16,128,256]{2,1,0:T(8,128)(2,1)S(1)} async-done(((bf16[16,128,256]{2,1,0:T(8,128)(2,1)}), bf16[16,128,256]{2,1,0:T(8,128)(2,1)S(1)}, u32[]{:S(2)}, u32[]{:S(2)}) %all-to-all-start.2) | async-done | bytes 1048608 | tf_op jit(solution)/shard_map/all_to_all | solution.py:21
  120.5 1.1 broadcast_in_dim.15
  121.5 7.9 %all-to-all-start.3 = ((bf16[16,256,128]{1,2,0:T(8,128)(2,1)}), bf16[16,256,128]{1,2,0:T(8,128)(2,1)S(1)}, u32[]{:S(2)}, u32[]{:S(2)}) async-start(bf16[16,256,128]{1,2,0:T(8,128)(2,1)} %broadcast_in_dim.15), calls=%async_computation.3 | async-start | bytes 2097152 | tf_op jit(solution)/shard_map/all_to_all | solution.py:21
  130.1 21.5 %all-to-all-done.3 = bf16[16,256,128]{1,2,0:T(8,128)(2,1)S(1)} async-done(((bf16[16,256,128]{1,2,0:T(8,128)(2,1)}), bf16[16,256,128]{1,2,0:T(8,128)(2,1)S(1)}, u32[]{:S(2)}, u32[]{:S(2)}) %all-to-all-start.3) | async-done | bytes 1048608 | tf_op jit(solution)/shard_map/all_to_all | solution.py:21
  151.6 1.2 broadcast_in_dim.12
  152.8 7.8 %all-to-all-start = ((bf16[16,128,256]{2,1,0:T(8,128)(2,1)}), bf16[16,128,256]{2,1,0:T(8,128)(2,1)}, u32[]{:S(2)}, u32[]{:S(2)}) async-start(bf16[16,128,256]{2,1,0:T(8,128)(2,1)} %broadcast_in_dim.12), calls=%async_computation | async-start | bytes 2097152 | tf_op jit(solution)/shard_map/all_to_all | solution.py:21
  161.2 3.2 fusion
  164.7 1.3 fusion.13
  166.0 1.3 fusion.12
  167.7 15.1 %all-to-all-done = bf16[16,128,256]{2,1,0:T(8,128)(2,1)} async-done(((bf16[16,128,256]{2,1,0:T(8,128)(2,1)}), bf16[16,128,256]{2,1,0:T(8,128)(2,1)}, u32[]{:S(2)}, u32[]{:S(2)}) %all-to-all-start) | async-done | bytes 1048608 | tf_op jit(solution)/shard_map/all_to_all | solution.py:21
  182.8 8.8 %convolution_convert_fusion = bf16[1024,2048]{1,0:T(8,128)(2,1)} fusion(bf16[256,2048]{0,1:T(8,128)(2,1)S(1)} %bitcast.55, f32[1024,256]{1,0:T(8,128)S(1)} %bitcast.58, bf16[2048,256]{1,0:T(8,128)(2,1)} %bitcast, bf16[1024,2048]{1,0:T(8,128)(2,1)} %all-gather.11.cloned.1.call-done, f32[2048]{0:T(1024)S(1)} %convert_element_type.79, ...), kind=kOutput, calls=%fused_computation.18 | convolution fusion | flops 2159017984 | bytes 11546624 | tf_op jit(solution)/shard_map/dot_general | solution.py:106
  191.7 2.5 copy.46
  194.1 56.0 %all_to_all.43 = bf16[8,1024,256]{2,1,0:T(8,128)(2,1)S(1)} all-to-all(bf16[8,1024,256]{2,1,0:T(8,128)(2,1)S(1)} %bitcast.44), channel_id=1, replica_groups=mesh['rep'=2,'fs_0'=4,'fs_1'=4,'tp'=8] {'tp'}, dimensions={0} | all-to-all | bytes 8388608 | tf_op jit(solution)/shard_map/all_to_all | solution.py:35
  251.6 4.2 %all-to-all-start.5 = ((f32[8,1,1024]{2,1,0:T(1,128)}), f32[8,1,1024]{2,1,0:T(1,128)S(1)}, u32[]{:S(2)}, u32[]{:S(2)}) async-start(f32[8,1,1024]{2,1,0:T(1,128)} %broadcast_in_dim.16), calls=%async_computation.5 | async-start | bytes 65536 | tf_op jit(solution)/shard_map/all_to_all | solution.py:21
  256.6 4.0 %all-to-all-done.5 = f32[8,1,1024]{2,1,0:T(1,128)S(1)} async-done(((f32[8,1,1024]{2,1,0:T(1,128)}), f32[8,1,1024]{2,1,0:T(1,128)S(1)}, u32[]{:S(2)}, u32[]{:S(2)}) %all-to-all-start.5) | async-done | bytes 32800 | tf_op jit(solution)/shard_map/all_to_all | solution.py:21
  260.6 1.1 add_convert_fusion.1
  261.8 4.5 %copy.35 = bf16[4,4,1024,128]{3,2,1,0:T(8,128)(2,1)} copy(bf16[4,4,1024,128]{3,2,0,1:T(8,128)(2,1)} %bitcast.47) | data formatting | bytes 8388608 | tf_op jit(solution)/shard_map/transpose | solution.py:50
  266.3 6.4 %copy.36 = bf16[1024,16,128]{0,2,1:T(8,128)(2,1)} copy(bf16[1024,16,128]{2,0,1:T(8,128)(2,1)} %bitcast.45) | data formatting | bytes 8388608 | tf_op jit(solution)/shard_map/transpose | solution.py:14
  272.7 5.0 %copy.34 = bf16[4,4,128,1024]{3,2,1,0:T(8,128)(2,1)} copy(bf16[4,4,128,1024]{3,2,0,1:T(8,128)(2,1)} %bitcast.48) | data formatting | bytes 8388608 | tf_op jit(solution)/shard_map/transpose | solution.py:50
  277.7 22.9 %all-gather.13.cloned.1.call-done = bf16[1024,2048]{1,0:T(8,128)(2,1)} async-done(((bf16[1024,256]{1,0:T(8,128)(2,1)}), bf16[1024,2048]{1,0:T(8,128)(2,1)}) %all-gather.13.cloned.1.call-update) | async-done | bytes 4194320 | tf_op jit(solution)/shard_map/all_gather | solution.py:114
  300.6 3.1 fusion.3
  303.7 14.6 %convolution_convert_fusion.1 = bf16[1024,2048]{1,0:T(8,128)(2,1)} fusion(bf16[1024,2048]{0,1:T(8,128)(2,1)} %bitcast.49, bf16[2048,1024]{1,0:T(8,128)(2,1)} %bitcast.50, bf16[1024,2048]{1,0:T(8,128)(2,1)} %all-gather.13.cloned.1.call-done, f32[2048]{0:T(1024)S(1)} %convert_element_type.95, f32[1024]{0:T(1024)S(1)} %add_rsqrt_fusion.1), kind=kOutput, calls=%fused_computation.19 | convolution fusion | flops 8603566080 | bytes 16789504 | tf_op jit(solution)/shard_map/dot_general | solution.py:118
  318.3 2.5 copy.45
  320.8 52.6 %all_to_all.44 = bf16[8,1024,256]{2,1,0:T(8,128)(2,1)S(1)} all-to-all(bf16[8,1024,256]{2,1,0:T(8,128)(2,1)S(1)} %bitcast.46), channel_id=1, replica_groups=mesh['rep'=2,'fs_0'=4,'fs_1'=4,'tp'=8] {'tp'}, dimensions={0} | all-to-all | bytes 8388608 | tf_op jit(solution)/shard_map/all_to_all | solution.py:35
  374.8 4.3 %all-to-all-start.7 = ((f32[8,1,1024]{2,1,0:T(1,128)}), f32[8,1,1024]{2,1,0:T(1,128)S(1)}, u32[]{:S(2)}, u32[]{:S(2)}) async-start(f32[8,1,1024]{2,1,0:T(1,128)} %broadcast_in_dim.17), calls=%async_computation.7 | async-start | bytes 65536 | tf_op jit(solution)/shard_map/all_to_all | solution.py:21
  379.9 4.0 %all-to-all-done.7 = f32[8,1,1024]{2,1,0:T(1,128)S(1)} async-done(((f32[8,1,1024]{2,1,0:T(1,128)}), f32[8,1,1024]{2,1,0:T(1,128)S(1)}, u32[]{:S(2)}, u32[]{:S(2)}) %all-to-all-start.7) | async-done | bytes 32800 | tf_op jit(solution)/shard_map/all_to_all | solution.py:21
  383.9 1.1 add_convert_fusion
  (52 shorter events, 8.7 us)
Async XLA Ops:
  6.5 81.1 %copy-start.3 = (bf16[128,256]{1,0:T(8,128)(2,1)S(1)}, bf16[128,256]{1,0:T(8,128)(2,1)}, u32[]{:S(2)}) copy-start(bf16[128,256]{1,0:T(8,128)(2,1)} %param.16) | copy-start | bytes 196612
  6.5 39.2 %all-gather.19.cloned.1.call-start = ((), (), s32[]{:S(2)}) async-start(), calls=%async_computation.12 | async-start | bytes 1310720 | tf_op jit(solution)/shard_map/all_gather | solution.py:47
  7.3 91.2 %copy-start.5 = (bf16[256,128]{1,0:T(8,128)(2,1)S(1)}, bf16[256,128]{1,0:T(8,128)(2,1)}, u32[]{:S(2)}) copy-start(bf16[256,128]{1,0:T(8,128)(2,1)} %param.18) | copy-start | bytes 196612
  7.3 153.4 %all-gather.15.cloned.1.call-start = ((), (), s32[]{:S(2)}) async-start(), calls=%async_computation.10 | async-start | bytes 1310720 | tf_op jit(solution)/shard_map/all_gather | solution.py:47
  8.0 153.2 %all-gather.11.cloned.1.call-start = ((), (), s32[]{:S(2)}) async-start(), calls=%async_computation.8 | async-start | bytes 4718592 | tf_op jit(solution)/shard_map/all_gather | solution.py:90
  8.8 253.0 %all-gather.21.cloned.1.call-start = ((), (), s32[]{:S(2)}) async-start(), calls=%async_computation.13 | async-start | bytes 5242880 | tf_op jit(solution)/shard_map/all_gather | solution.py:47
  46.7 104.9 %copy-start.4 = (bf16[128,256]{1,0:T(8,128)(2,1)S(1)}, bf16[128,256]{1,0:T(8,128)(2,1)}, u32[]{:S(2)}) copy-start(bf16[128,256]{1,0:T(8,128)(2,1)} %param.14) | copy-start | bytes 196612
  88.7 72.0 %copy-start.6 = (bf16[2048]{0:T(1024)(128)(2,1)S(1)}, bf16[2048]{0:T(1024)(128)(2,1)}, u32[]{:S(2)}) copy-start(bf16[2048]{0:T(1024)(128)(2,1)} %param.13) | copy-start | bytes 12292
  88.7 31.8 %all-to-all-start.2 = ((bf16[16,128,256]{2,1,0:T(8,128)(2,1)}), bf16[16,128,256]{2,1,0:T(8,128)(2,1)S(1)}, u32[]{:S(2)}, u32[]{:S(2)}) async-start(bf16[16,128,256]{2,1,0:T(8,128)(2,1)} %broadcast_in_dim.14), calls=%async_computation.2 | async-start | bytes 2097152 | tf_op jit(solution)/shard_map/all_to_all | solution.py:21
  121.5 30.1 %all-to-all-start.3 = ((bf16[16,256,128]{1,2,0:T(8,128)(2,1)}), bf16[16,256,128]{1,2,0:T(8,128)(2,1)S(1)}, u32[]{:S(2)}, u32[]{:S(2)}) async-start(bf16[16,256,128]{1,2,0:T(8,128)(2,1)} %broadcast_in_dim.15), calls=%async_computation.3 | async-start | bytes 2097152 | tf_op jit(solution)/shard_map/all_to_all | solution.py:21
  152.8 30.1 %all-to-all-start = ((bf16[16,128,256]{2,1,0:T(8,128)(2,1)}), bf16[16,128,256]{2,1,0:T(8,128)(2,1)}, u32[]{:S(2)}, u32[]{:S(2)}) async-start(bf16[16,128,256]{2,1,0:T(8,128)(2,1)} %broadcast_in_dim.12), calls=%async_computation | async-start | bytes 2097152 | tf_op jit(solution)/shard_map/all_to_all | solution.py:21
  160.6 112.1 %all-gather.17.cloned.1.call-start = ((), (), s32[]{:S(2)}) async-start(), calls=%async_computation.11 | async-start | bytes 5242880 | tf_op jit(solution)/shard_map/all_gather | solution.py:47
  161.2 3.5 copy-start.1
  250.2 10.5 %copy-start.2 = (bf16[1024,256]{1,0:T(8,128)(2,1)S(1)}, bf16[1024,256]{1,0:T(8,128)(2,1)}, u32[]{:S(2)}) copy-start(bf16[1024,256]{1,0:T(8,128)(2,1)} %param.12) | copy-start | bytes 1572868
  250.2 11.5 %copy-start.7 = (bf16[2048]{0:T(1024)(128)(2,1)S(1)}, bf16[2048]{0:T(1024)(128)(2,1)}, u32[]{:S(2)}) copy-start(bf16[2048]{0:T(1024)(128)(2,1)} %param.20) | copy-start | bytes 12292
  251.6 9.0 %all-to-all-start.5 = ((f32[8,1,1024]{2,1,0:T(1,128)}), f32[8,1,1024]{2,1,0:T(1,128)S(1)}, u32[]{:S(2)}, u32[]{:S(2)}) async-start(f32[8,1,1024]{2,1,0:T(1,128)} %broadcast_in_dim.16), calls=%async_computation.5 | async-start | bytes 65536 | tf_op jit(solution)/shard_map/all_to_all | solution.py:21
  255.8 44.7 %all-gather.13.cloned.1.call-start = ((), (), s32[]{:S(2)}) async-start(), calls=%async_computation.9 | async-start | bytes 4718592 | tf_op jit(solution)/shard_map/all_gather | solution.py:114
  373.4 10.5 %copy-start = (bf16[1024,256]{1,0:T(8,128)(2,1)S(1)}, bf16[1024,256]{1,0:T(8,128)(2,1)}, u32[]{:S(2)}) copy-start(bf16[1024,256]{1,0:T(8,128)(2,1)} %add_convert_fusion.1) | copy-start | bytes 1572868
  374.8 9.0 %all-to-all-start.7 = ((f32[8,1,1024]{2,1,0:T(1,128)}), f32[8,1,1024]{2,1,0:T(1,128)S(1)}, u32[]{:S(2)}, u32[]{:S(2)}) async-start(f32[8,1,1024]{2,1,0:T(1,128)} %broadcast_in_dim.17), calls=%async_computation.7 | async-start | bytes 65536 | tf_op jit(solution)/shard_map/all_to_all | solution.py:21
Sparse Core Ops, SparseCore 0:
  9.1 36.5 all-gather.18
  47.5 43.0 all-gather.14
  92.5 42.0 all-gather.10
  136.3 62.9 all-gather.20
  200.9 51.1 all-gather.16
  261.8 38.7 all-gather.12
where the time goes:
time: 393 us; the launch traced here: 392 us
  blocking collectives  150 us (38%)
  waiting for transfers between devices  129 us (33%)
  starting transfers between devices  34.2 us (9%)
  local copies, waits for them, and re-layouts  26.7 us (7%)
  matrix products  26.1 us (7%)
  between operations  13.7 us (3%)
  other arithmetic  12.6 us (3%)
    all_to_all x2, blocking collectives, sent_and_summed(): lax.all_to_all(pieces, axis, split_axis=0, concat_axis=0, tiled=True)  109 us
    all_to_all x5, waiting for transfers between devices, from_everyone(): lax.all_to_all(jnp.broadcast_to(x[None], (length, *x.shape)), axis, 0, 0,...  66.4 us
    all_to_all x1, blocking collectives, from_everyone(): lax.all_to_all(jnp.broadcast_to(x[None], (length, *x.shape)), axis, 0, 0,...  40.9 us
    all_gather x4, waiting for transfers between devices, all_blocks(): pieces = lax.all_gather(pieces, axes[k])  37 us
    all_to_all x5, starting transfers between devices, from_everyone(): lax.all_to_all(jnp.broadcast_to(x[None], (length, *x.shape)), axis, 0, 0,...  34 us
    all_gather x1, waiting for transfers between devices, body(): resid = lax.all_gather(resid_own, 'tp', axis=1, tiled=True)  22.9 us
    dot_general x1, matrix products, body(): jnp.dot(active, whole_of(down_weight, FS, (0, 1), 1), preferred_element_t...  14.6 us
    transpose x2, local copies, waits for them, and re-layouts, all_blocks(): pieces = pieces.transpose(*back, *range(len(axes), pieces.ndim))  9.5 us
  transfers between devices with their start and end apart: 11, of which 7 were waited for; matrix products, arithmetic and copies ran while one was open for 11% of the time, Pallas kernels for 0%

commit v1 on v0

--- a/solution.py
+++ b/solution.py
@@ -111,7 +111,9 @@
     gain_own = lax.dynamic_slice_in_dim(mix_out_gain, first, own_width, 0).astype(jnp.float32)
     scaled = mixed * lax.rsqrt(power[:, None] / full_width + epsilon) * gain_own
     resid_own = (tokens.astype(jnp.float32) + scaled).astype(jnp.bfloat16)
-    resid = lax.all_gather(resid_own, "tp", axis=1, tiled=True)
+    resid = jnp.concatenate(
+        lax.all_to_all(jnp.stack([resid_own] * lax.axis_size("tp")), "tp", 0, 0), axis=1
+    )
     second = normalize(resid, ffn_in_gain).astype(jnp.bfloat16)
     lifted = jnp.dot(second, whole_of(up_weight, FS, (0, 1), 0), preferred_element_type=jnp.float32)
     active = jnp.square(jnp.maximum(lifted, 0.0)).astype(jnp.bfloat16)

time: 393 us -> 397 us (1.010)
  blocking collectives: 150 us -> 97.9 us
  starting transfers between devices: 34.2 us -> 61.6 us
  waiting for transfers between devices: 129 us -> 146 us
  other arithmetic: 12.6 us -> 18.3 us
  local copies, waits for them, and re-layouts: 26.7 us -> 31.9 us
    all_to_all x0 -> x2, waiting for transfers between devices: none -> 81.3 us  [the longest x1 48.2 us: sent_and_summed(): lax.all_to_all(pieces, axis, split_axis=0, concat_axis=0, tiled=True)]
    all_to_all x2 -> x1, blocking collectives: 109 us -> 52.1 us  [sent_and_summed(): lax.all_to_all(pieces, axis, split_axis=0, concat_axis=0, tiled=True)]
    all_gather x4, waiting for transfers between devices: 37 us -> 0.05 us  [all_blocks(): pieces = lax.all_gather(pieces, axes[k])]
    all_gather x1 -> x0, waiting for transfers between devices: 22.9 us -> none  [body(): resid = lax.all_gather(resid_own, 'tp', axis=1, tiled=True)]
    all_to_all x0 -> x2, starting transfers between devices: none -> 18.7 us  [the longest x1 13.4 us: sent_and_summed(): lax.all_to_all(pieces, axis, split_axis=0, concat_axis=0, tiled=True)]
    all_to_all x5, starting transfers between devices: 34 us -> 42.8 us  [from_everyone(): lax.all_to_all(jnp.broadcast_to(x[None], (length, *x.shape)), axis, 0, 0,...]
    all_to_all x1, blocking collectives: 40.9 us -> 45.8 us  [from_everyone(): lax.all_to_all(jnp.broadcast_to(x[None], (length, *x.shape)), axis, 0, 0,...]
    all_to_all x5, waiting for transfers between devices: 66.4 us -> 61.7 us  [from_everyone(): lax.all_to_all(jnp.broadcast_to(x[None], (length, *x.shape)), axis, 0, 0,...]
  transfers between devices with their start and end apart: 11 -> 12, of which waited for: 7 -> 7; matrix products, arithmetic and copies ran while one was open for 11% -> 13% of each run, Pallas kernels for 0% -> 0%
where the time goes in v1:
time: 397 us; the launch traced here: 395 us
  waiting for transfers between devices  146 us (37%)
  blocking collectives  97.9 us (25%)
  starting transfers between devices  61.6 us (16%)
  local copies, waits for them, and re-layouts  31.9 us (8%)
  matrix products  26.2 us (7%)
  other arithmetic  18.3 us (5%)
  between operations  13.4 us (3%)
    all_to_all x5, waiting for transfers between devices, from_everyone(): lax.all_to_all(jnp.broadcast_to(x[None], (length, *x.shape)), axis, 0, 0,...  61.7 us
    all_to_all x1, blocking collectives, sent_and_summed(): lax.all_to_all(pieces, axis, split_axis=0, concat_axis=0, tiled=True)  52.1 us
    all_to_all x1, waiting for transfers between devices, sent_and_summed(): lax.all_to_all(pieces, axis, split_axis=0, concat_axis=0, tiled=True)  48.2 us
    all_to_all x1, blocking collectives, from_everyone(): lax.all_to_all(jnp.broadcast_to(x[None], (length, *x.shape)), axis, 0, 0,...  45.8 us
    all_to_all x5, starting transfers between devices, from_everyone(): lax.all_to_all(jnp.broadcast_to(x[None], (length, *x.shape)), axis, 0, 0,...  42.8 us
    all_to_all x1, waiting for transfers between devices, body(): lax.all_to_all(jnp.stack([resid_own] * lax.axis_size('tp')), 'tp', 0, 0)  33.1 us
    dot_general x1, matrix products, body(): jnp.dot(active, whole_of(down_weight, FS, (0, 1), 1), preferred_element_t...  14.4 us
    all_to_all x1, starting transfers between devices, sent_and_summed(): lax.all_to_all(pieces, axis, split_axis=0, concat_axis=0, tiled=True)  13.4 us
  transfers between devices with their start and end apart: 12, of which 7 were waited for; matrix products, arithmetic and copies ran while one was open for 13% of the time, Pallas kernels for 0%

profile of v1, /device:TPU:1, one launch (start us, length us, event | category | flops | bytes accessed | tf_op | source)
XLA Modules:
  0.0 395.4 jit_solution(11568937748411543078)
XLA Ops:
  8.9 45.8 %all_to_all.47 = bf16[16,128,256]{2,1,0:T(8,128)(2,1)S(1)} all-to-all(bf16[16,128,256]{2,1,0:T(8,128)(2,1)S(1)} %broadcast_in_dim.13), channel_id=1, replica_groups=mesh['rep'=2,'fs_0'=4,'fs_1'=4,'tp'=8] {'fs_0','fs_1'}, dimensions={0} | all-to-all | bytes 2097152 | tf_op jit(solution)/shard_map/all_to_all | solution.py:21
  54.7 2.0 broadcast_in_dim.14
  56.7 9.1 %all-to-all-start.2 = ((bf16[16,128,256]{2,1,0:T(8,128)(2,1)}), bf16[16,128,256]{2,1,0:T(8,128)(2,1)S(1)}, u32[]{:S(2)}, u32[]{:S(2)}) async-start(bf16[16,128,256]{2,1,0:T(8,128)(2,1)} %broadcast_in_dim.14), calls=%async_computation.2 | async-start | bytes 2097152 | tf_op jit(solution)/shard_map/all_to_all | solution.py:21
  66.7 21.3 %all-to-all-done.2 = bf16[16,128,256]{2,1,0:T(8,128)(2,1)S(1)} async-done(((bf16[16,128,256]{2,1,0:T(8,128)(2,1)}), bf16[16,128,256]{2,1,0:T(8,128)(2,1)S(1)}, u32[]{:S(2)}, u32[]{:S(2)}) %all-to-all-start.2) | async-done | bytes 1048608 | tf_op jit(solution)/shard_map/all_to_all | solution.py:21
  88.0 1.1 broadcast_in_dim.15
  89.1 7.9 %all-to-all-start.3 = ((bf16[16,256,128]{1,2,0:T(8,128)(2,1)}), bf16[16,256,128]{1,2,0:T(8,128)(2,1)S(1)}, u32[]{:S(2)}, u32[]{:S(2)}) async-start(bf16[16,256,128]{1,2,0:T(8,128)(2,1)} %broadcast_in_dim.15), calls=%async_computation.3 | async-start | bytes 2097152 | tf_op jit(solution)/shard_map/all_to_all | solution.py:21
  98.2 20.9 %all-to-all-done.3 = bf16[16,256,128]{1,2,0:T(8,128)(2,1)S(1)} async-done(((bf16[16,256,128]{1,2,0:T(8,128)(2,1)}), bf16[16,256,128]{1,2,0:T(8,128)(2,1)S(1)}, u32[]{:S(2)}, u32[]{:S(2)}) %all-to-all-start.3) | async-done | bytes 1048608 | tf_op jit(solution)/shard_map/all_to_all | solution.py:21
  120.2 17.2 %all-to-all-start = ((bf16[16,128,256]{2,1,0:T(8,128)(2,1)}), bf16[16,128,256]{2,1,0:T(8,128)(2,1)}, u32[]{:S(2)}, u32[]{:S(2)}) async-start(bf16[16,128,256]{2,1,0:T(8,128)(2,1)} %broadcast_in_dim.12), calls=%async_computation | async-start | bytes 2097152 | tf_op jit(solution)/shard_map/all_to_all | solution.py:21
  137.6 3.2 fusion
  141.0 1.3 fusion.8
  142.3 1.3 fusion.7
  143.9 11.6 %all-to-all-done = bf16[16,128,256]{2,1,0:T(8,128)(2,1)} async-done(((bf16[16,128,256]{2,1,0:T(8,128)(2,1)}), bf16[16,128,256]{2,1,0:T(8,128)(2,1)}, u32[]{:S(2)}, u32[]{:S(2)}) %all-to-all-start) | async-done | bytes 1048608 | tf_op jit(solution)/shard_map/all_to_all | solution.py:21
  155.5 9.2 %convolution_convert_fusion = bf16[1024,2048]{1,0:T(8,128)(2,1)} fusion(bf16[256,2048]{0,1:T(8,128)(2,1)S(1)} %bitcast.62, f32[1024,256]{1,0:T(8,128)S(1)} %bitcast.63, bf16[2048,256]{1,0:T(8,128)(2,1)} %bitcast, bf16[1024,2048]{1,0:T(8,128)(2,1)} %all-gather.10.cloned.1.call-done, f32[2048]{0:T(1024)S(1)} %convert_element_type.86, ...), kind=kOutput, calls=%fused_computation.15 | convolution fusion | flops 2159017984 | bytes 11546624 | tf_op jit(solution)/shard_map/dot_general | solution.py:106
  164.7 4.4 %copy.51 = bf16[128,8,8,256]{3,2,0,1:T(8,128)(2,1)} copy(bf16[128,8,8,256]{3,2,1,0:T(8,128)(2,1)} %bitcast.55) | data formatting | bytes 8388608 | tf_op jit(solution)/shard_map/reshape | solution.py:30
  169.1 13.4 %all-to-all-start.4 = ((bf16[8,1024,256]{2,1,0:T(8,128)(2,1)}), bf16[8,1024,256]{2,1,0:T(8,128)(2,1)}, u32[]{:S(2)}, u32[]{:S(2)}) async-start(bf16[8,1024,256]{2,1,0:T(8,128)(2,1)} %bitcast.48), calls=%async_computation.4 | async-start | bytes 8388608 | tf_op jit(solution)/shard_map/all_to_all | solution.py:35
  183.0 48.2 %all-to-all-done.4 = bf16[8,1024,256]{2,1,0:T(8,128)(2,1)} async-done(((bf16[8,1024,256]{2,1,0:T(8,128)(2,1)}), bf16[8,1024,256]{2,1,0:T(8,128)(2,1)}, u32[]{:S(2)}, u32[]{:S(2)}) %all-to-all-start.4) | async-done | bytes 4194336 | tf_op jit(solution)/shard_map/all_to_all | solution.py:35
  231.2 2.9 convert_reduce_fusion.1
  235.0 4.2 %all-to-all-start.5 = ((f32[8,1,1024]{2,1,0:T(1,128)}), f32[8,1,1024]{2,1,0:T(1,128)S(1)}, u32[]{:S(2)}, u32[]{:S(2)}) async-start(f32[8,1,1024]{2,1,0:T(1,128)} %broadcast_in_dim.16), calls=%async_computation.5 | async-start | bytes 65536 | tf_op jit(solution)/shard_map/all_to_all | solution.py:21
  240.0 4.0 %all-to-all-done.5 = f32[8,1,1024]{2,1,0:T(1,128)S(1)} async-done(((f32[8,1,1024]{2,1,0:T(1,128)}), f32[8,1,1024]{2,1,0:T(1,128)S(1)}, u32[]{:S(2)}, u32[]{:S(2)}) %all-to-all-start.5) | async-done | bytes 32800 | tf_op jit(solution)/shard_map/all_to_all | solution.py:21
  244.6 2.5 stack.2
  247.0 5.3 %all-to-all-start.6 = ((bf16[8,1024,256]{1,2,0:T(8,128)(2,1)}), bf16[8,1024,256]{1,2,0:T(8,128)(2,1)}, u32[]{:S(2)}, u32[]{:S(2)}) async-start(bf16[8,1024,256]{1,2,0:T(8,128)(2,1)} %stack.2), calls=%async_computation.6 | async-start | bytes 8388608 | tf_op jit(solution)/shard_map/all_to_all | solution.py:115
  252.3 4.5 %copy.40 = bf16[4,4,1024,128]{3,2,1,0:T(8,128)(2,1)} copy(bf16[4,4,1024,128]{3,2,0,1:T(8,128)(2,1)} %bitcast.51) | data formatting | bytes 8388608 | tf_op jit(solution)/shard_map/transpose | solution.py:50
  256.9 6.4 %copy.41 = bf16[1024,16,128]{0,2,1:T(8,128)(2,1)} copy(bf16[1024,16,128]{2,0,1:T(8,128)(2,1)} %bitcast.49) | data formatting | bytes 8388608 | tf_op jit(solution)/shard_map/transpose | solution.py:14
  263.3 4.7 %copy.39 = bf16[4,4,128,1024]{3,2,1,0:T(8,128)(2,1)} copy(bf16[4,4,128,1024]{3,2,0,1:T(8,128)(2,1)} %bitcast.52) | data formatting | bytes 8388608 | tf_op jit(solution)/shard_map/transpose | solution.py:50
  268.0 33.1 %all-to-all-done.6 = bf16[8,1024,256]{1,2,0:T(8,128)(2,1)} async-done(((bf16[8,1024,256]{1,2,0:T(8,128)(2,1)}), bf16[8,1024,256]{1,2,0:T(8,128)(2,1)}, u32[]{:S(2)}, u32[]{:S(2)}) %all-to-all-start.6) | async-done | bytes 4194336 | tf_op jit(solution)/shard_map/all_to_all | solution.py:115
  301.1 3.1 fusion.3
  304.2 4.1 %fusion.5 = bf16[8,1024,256]{1,2,0:T(8,128)(2,1)} fusion(bf16[8,1024,256]{1,2,0:T(8,128)(2,1)} %all-to-all-done.6, f32[8,256]{1,0:T(8,128)S(1)} %reshape.111, f32[1024]{0:T(1024)S(1)} %add_rsqrt_fusion.1), kind=kLoop, calls=%fused_computation.9 | loop fusion | flops 8388608 | bytes 8400896 | tf_op jit(solution)/shard_map/convert_element_type | solution.py:117
  308.3 14.4 %convolution_convert_fusion.1 = bf16[1024,2048]{1,0:T(8,128)(2,1)} fusion(bf16[1024,2048]{0,1:T(8,128)(2,1)} %bitcast.53, bf16[1024,2048]{0,1:T(8,128)(2,1)} %bitcast.56, bf16[2048,1024]{1,0:T(8,128)(2,1)} %bitcast.54), kind=kOutput, calls=%fused_computation.16 | convolution fusion | flops 8595177472 | bytes 16777216 | tf_op jit(solution)/shard_map/dot_general | solution.py:120
  322.7 2.5 copy.50
  325.2 52.1 %all_to_all.48 = bf16[8,1024,256]{2,1,0:T(8,128)(2,1)S(1)} all-to-all(bf16[8,1024,256]{2,1,0:T(8,128)(2,1)S(1)} %bitcast.50), channel_id=1, replica_groups=mesh['rep'=2,'fs_0'=4,'fs_1'=4,'tp'=8] {'tp'}, dimensions={0} | all-to-all | bytes 8388608 | tf_op jit(solution)/shard_map/all_to_all | solution.py:35
  378.7 4.3 %all-to-all-start.8 = ((f32[8,1,1024]{2,1,0:T(1,128)}), f32[8,1,1024]{2,1,0:T(1,128)S(1)}, u32[]{:S(2)}, u32[]{:S(2)}) async-start(f32[8,1,1024]{2,1,0:T(1,128)} %broadcast_in_dim.17), calls=%async_computation.8 | async-start | bytes 65536 | tf_op jit(solution)/shard_map/all_to_all | solution.py:21
  383.7 4.0 %all-to-all-done.8 = f32[8,1,1024]{2,1,0:T(1,128)S(1)} async-done(((f32[8,1,1024]{2,1,0:T(1,128)}), f32[8,1,1024]{2,1,0:T(1,128)S(1)}, u32[]{:S(2)}, u32[]{:S(2)}) %all-to-all-start.8) | async-done | bytes 32800 | tf_op jit(solution)/shard_map/all_to_all | solution.py:21
  (51 shorter events, 12.1 us)
Async XLA Ops:
  6.5 60.1 %copy-start.3 = (bf16[256,128]{1,0:T(8,128)(2,1)S(1)}, bf16[256,128]{1,0:T(8,128)(2,1)}, u32[]{:S(2)}) copy-start(bf16[256,128]{1,0:T(8,128)(2,1)} %param.18) | copy-start | bytes 196612
  6.5 90.5 %all-gather.16.cloned.1.call-start = ((), (), s32[]{:S(2)}) async-start(), calls=%async_computation.12 | async-start | bytes 1310720 | tf_op jit(solution)/shard_map/all_gather | solution.py:47
  7.3 130.3 %all-gather.10.cloned.1.call-start = ((), (), s32[]{:S(2)}) async-start(), calls=%async_computation.9 | async-start | bytes 4718592 | tf_op jit(solution)/shard_map/all_gather | solution.py:90
  54.7 64.4 %copy-start.2 = (bf16[128,256]{1,0:T(8,128)(2,1)S(1)}, bf16[128,256]{1,0:T(8,128)(2,1)}, u32[]{:S(2)}) copy-start(bf16[128,256]{1,0:T(8,128)(2,1)} %param.14) | copy-start | bytes 196612
  56.7 31.3 %all-to-all-start.2 = ((bf16[16,128,256]{2,1,0:T(8,128)(2,1)}), bf16[16,128,256]{2,1,0:T(8,128)(2,1)S(1)}, u32[]{:S(2)}, u32[]{:S(2)}) async-start(bf16[16,128,256]{2,1,0:T(8,128)(2,1)} %broadcast_in_dim.14), calls=%async_computation.2 | async-start | bytes 2097152 | tf_op jit(solution)/shard_map/all_to_all | solution.py:21
  65.9 71.6 %copy-start.4 = (bf16[2048]{0:T(1024)(128)(2,1)S(1)}, bf16[2048]{0:T(1024)(128)(2,1)}, u32[]{:S(2)}) copy-start(bf16[2048]{0:T(1024)(128)(2,1)} %param.13) | copy-start | bytes 12292
  65.9 116.6 %all-gather.12.cloned.1.call-start = ((), (), s32[]{:S(2)}) async-start(), calls=%async_computation.10 | async-start | bytes 1310720 | tf_op jit(solution)/shard_map/all_gather | solution.py:47
  89.1 30.1 %all-to-all-start.3 = ((bf16[16,256,128]{1,2,0:T(8,128)(2,1)}), bf16[16,256,128]{1,2,0:T(8,128)(2,1)S(1)}, u32[]{:S(2)}, u32[]{:S(2)}) async-start(bf16[16,256,128]{1,2,0:T(8,128)(2,1)} %broadcast_in_dim.15), calls=%async_computation.3 | async-start | bytes 2097152 | tf_op jit(solution)/shard_map/all_to_all | solution.py:21
  97.0 155.3 %all-gather.18.cloned.1.call-start = ((), (), s32[]{:S(2)}) async-start(), calls=%async_computation.13 | async-start | bytes 5242880 | tf_op jit(solution)/shard_map/all_gather | solution.py:47
  120.2 35.3 %all-to-all-start = ((bf16[16,128,256]{2,1,0:T(8,128)(2,1)}), bf16[16,128,256]{2,1,0:T(8,128)(2,1)}, u32[]{:S(2)}, u32[]{:S(2)}) async-start(bf16[16,128,256]{2,1,0:T(8,128)(2,1)} %broadcast_in_dim.12), calls=%async_computation | async-start | bytes 2097152 | tf_op jit(solution)/shard_map/all_to_all | solution.py:21
  137.5 3.5 copy-start
  169.1 62.2 %all-to-all-start.4 = ((bf16[8,1024,256]{2,1,0:T(8,128)(2,1)}), bf16[8,1024,256]{2,1,0:T(8,128)(2,1)}, u32[]{:S(2)}, u32[]{:S(2)}) async-start(bf16[8,1024,256]{2,1,0:T(8,128)(2,1)} %bitcast.48), calls=%async_computation.4 | async-start | bytes 8388608 | tf_op jit(solution)/shard_map/all_to_all | solution.py:35
  182.5 61.6 %copy-start.1 = (bf16[1024,256]{1,0:T(8,128)(2,1)S(1)}, bf16[1024,256]{1,0:T(8,128)(2,1)}, u32[]{:S(2)}) copy-start(bf16[1024,256]{1,0:T(8,128)(2,1)} %param.12) | copy-start | bytes 1572868
  182.5 80.8 %all-gather.14.cloned.1.call-start = ((), (), s32[]{:S(2)}) async-start(), calls=%async_computation.11 | async-start | bytes 5242880 | tf_op jit(solution)/shard_map/all_gather | solution.py:47
  235.0 9.0 %all-to-all-start.5 = ((f32[8,1,1024]{2,1,0:T(1,128)}), f32[8,1,1024]{2,1,0:T(1,128)S(1)}, u32[]{:S(2)}, u32[]{:S(2)}) async-start(f32[8,1,1024]{2,1,0:T(1,128)} %broadcast_in_dim.16), calls=%async_computation.5 | async-start | bytes 65536 | tf_op jit(solution)/shard_map/all_to_all | solution.py:21
  247.0 5.3 %copy-start.5 = (bf16[2048]{0:T(1024)(128)(2,1)S(1)}, bf16[2048]{0:T(1024)(128)(2,1)}, u32[]{:S(2)}) copy-start(bf16[2048]{0:T(1024)(128)(2,1)} %param.20) | copy-start | bytes 12292
  247.0 54.1 %all-to-all-start.6 = ((bf16[8,1024,256]{1,2,0:T(8,128)(2,1)}), bf16[8,1024,256]{1,2,0:T(8,128)(2,1)}, u32[]{:S(2)}, u32[]{:S(2)}) async-start(bf16[8,1024,256]{1,2,0:T(8,128)(2,1)} %stack.2), calls=%async_computation.6 | async-start | bytes 8388608 | tf_op jit(solution)/shard_map/all_to_all | solution.py:115
  378.7 9.0 %all-to-all-start.8 = ((f32[8,1,1024]{2,1,0:T(1,128)}), f32[8,1,1024]{2,1,0:T(1,128)S(1)}, u32[]{:S(2)}, u32[]{:S(2)}) async-start(f32[8,1,1024]{2,1,0:T(1,128)} %broadcast_in_dim.17), calls=%async_computation.8 | async-start | bytes 65536 | tf_op jit(solution)/shard_map/all_to_all | solution.py:21
Sparse Core Ops, SparseCore 0:
  9.1 47.4 all-gather.15
  58.4 41.5 all-gather.9
  101.9 37.4 all-gather.11
  141.0 52.7 all-gather.17
  195.5 52.1 all-gather.13
